TPU v7x, 32 devices: a whole 2x2x4 slice. The times are simulated.
32 devices in a mesh: sp: 8 (over z, x), tp: 4 (over y, core).
Axes of the slice: x: 2, y: 2, z: 4, core: 2. Of those that a mesh axis runs over, the one named last changes fastest.
Arguments:
- glu_value: bfloat16 [1024, 2048], P('tp', 'sp')
- glu_gate: bfloat16 [1024, 2048], P('tp', 'sp'), may hold values from -8 to 8
- conv_taps: float32 [1024, 31], P('tp'), may hold values from -1 to 1
- norm_gain: float32 [1024], P('tp'), may hold values from 0.1 to 1.9
- out_proj: bfloat16 [1024, 2048], P(None, 'tp'), may hold values from -0.1875 to 0.1875
- resid: bfloat16 [2048, 2048], P('sp', 'tp'), may hold values from -6 to 6
- expert_ids: int32 [2048, 2], P('sp'), may hold values from 0 to 7, all different within a row; in each aligned block of 256 rows (0 to 255, 256 to 511, ...) at most 128 rows name the same one
- route_logits: float32 [2048, 2], P('sp'), may hold values from -8 to 8
- group_prob: float32 [2048], P('sp'), may hold values from 0.2 to 1
- w_gate: bfloat16 [8, 2048, 4096], P('sp', None, 'tp'), may hold values from -0.125 to 0.125
- w_up: bfloat16 [8, 2048, 4096], P('sp', None, 'tp'), may hold values from -0.125 to 0.125
- w_down: bfloat16 [8, 4096, 2048], P('sp', None, 'tp'), may hold values from -0.09375 to 0.09375
Outputs:
- layer_out: bfloat16 [2048, 2048], P('sp', 'tp')
Inputs may be any that keep to these rules, and one draw needn't show every extreme that they name: `expert_ids`: each row names 2 different experts. In each aligned block of 256 rows (the rows of one index of sp) no expert is named by more than 128 rows, a bound that some block reaches.
All inputs are finite; a program needn't handle non-finite values.
Results may differ from a plain program's by a relative error of at most 0.0061.
Values may be sent and summed in bfloat16 or wider, within the bound.
A program may use at most 64 MiB of HBM per device.

v0:
```python
import jax
import jax.numpy as jnp
from jax import lax
from jax.sharding import PartitionSpec as P


def from_behind(block, axis, distance):
    devices = range(lax.axis_size(axis))
    route = [(i - distance, i) for i in devices if i - distance in devices]
    return lax.ppermute(block, axis, route)


def per_device(
    glu_value,
    glu_gate,
    conv_taps,
    norm_gain,
    out_proj,
    resid,
    expert_ids,
    route_logits,
    group_prob,
    w_gate,
    w_up,
    w_down,
):
    local_tokens = glu_value.shape[1]
    tap_count = conv_taps.shape[1]
    channels = glu_value.shape[0] * lax.axis_size("tp")
    gated = (glu_value.astype(jnp.float32) * jax.nn.sigmoid(glu_gate.astype(jnp.float32))).astype(
        jnp.bfloat16
    )
    history = from_behind(gated[:, local_tokens - (tap_count - 1) :], "sp", 1)
    padded = jnp.concatenate([history, gated], axis=1).astype(jnp.float32)
    filtered = jnp.zeros(gated.shape, jnp.float32)
    for offset in range(tap_count):
        filtered = (
            filtered + conv_taps[:, offset : offset + 1] * padded[:, offset : offset + local_tokens]
        )
    total_one, total_two = lax.psum(
        (jnp.sum(filtered, axis=0), jnp.sum(filtered * filtered, axis=0)), "tp"
    )
    mean = total_one / channels
    var = total_two / channels - mean * mean
    normed = (filtered - mean[None, :]) * lax.rsqrt(var[None, :] + 1e-05) * norm_gain[:, None]
    activated = jax.nn.silu(normed).astype(jnp.bfloat16)
    weights = out_proj
    projected = lax.dot_general(
        lax.all_gather(activated, "tp", axis=0, tiled=True),
        weights,
        (((0,), (0,)), ((), ())),
        preferred_element_type=jnp.float32,
    )
    mixed = (resid.astype(jnp.float32) + projected).astype(jnp.bfloat16)
    experts = lax.axis_size("sp")
    capacity = 4 * local_tokens // experts
    flat_ids = expert_ids.reshape(-1)
    onehot = (flat_ids[:, None] == jnp.arange(experts, dtype=jnp.int32)[None, :]).astype(jnp.int32)
    rank = jnp.sum(jnp.cumsum(onehot, axis=0) * onehot, axis=1) - 1
    slot = flat_ids * capacity + rank
    token_of = jnp.arange(flat_ids.shape[0], dtype=jnp.int32) // expert_ids.shape[1]
    table = jnp.zeros((experts * capacity,), jnp.int32).at[slot].set(token_of)
    filled = jnp.zeros((experts * capacity,), jnp.bool_).at[slot].set(True)
    route_weight = (group_prob[:, None] * jax.nn.softmax(route_logits, axis=-1)).reshape(-1)
    outgoing = jnp.where(
        filled[:, None], jnp.take(mixed, table, axis=0), jnp.zeros((), jnp.bfloat16)
    )
    outgoing = outgoing.reshape(experts, capacity, mixed.shape[1])
    rows = lax.all_gather(
        lax.all_to_all(outgoing, "sp", split_axis=0, concat_axis=0, tiled=True),
        "tp",
        axis=2,
        tiled=True,
    )
    sources, count, width = rows.shape
    flat_rows = rows.reshape(sources * count, width)
    gate_part = jnp.dot(flat_rows, w_gate[0], preferred_element_type=jnp.float32)
    up_part = jnp.dot(flat_rows, w_up[0], preferred_element_type=jnp.float32)
    hidden = (jax.nn.silu(gate_part) * up_part).astype(jnp.bfloat16)
    weights = w_down[0]
    expert_out = jnp.dot(
        lax.all_gather(hidden, "tp", axis=1, tiled=True),
        weights,
        preferred_element_type=jnp.float32,
    )
    results = expert_out.astype(jnp.bfloat16).reshape(sources, count, w_down.shape[2])
    returned = lax.all_to_all(results, "sp", split_axis=0, concat_axis=0, tiled=True)
    flat_back = returned.reshape(experts * capacity, returned.shape[2])
    picked = jnp.take(flat_back, slot, axis=0).astype(jnp.float32) * route_weight[:, None]
    routed = jnp.sum(picked.reshape(local_tokens, expert_ids.shape[1], flat_back.shape[1]), axis=1)
    return (mixed.astype(jnp.float32) + routed).astype(jnp.bfloat16)


def solution(mesh):
    return jax.shard_map(
        per_device,
        mesh=mesh,
        in_specs=(
            P("tp", "sp"),
            P("tp", "sp"),
            P("tp", None),
            P("tp"),
            P(None, "tp"),
            P("sp", "tp"),
            P("sp", None),
            P("sp", None),
            P("sp"),
            P("sp", None, "tp"),
            P("sp", None, "tp"),
            P("sp", None, "tp"),
        ),
        out_specs=P("sp", "tp"),
        check_vma=False,
    )
```

profile of v0, /device:TPU:0, one launch (start us, length us, event | category | flops | bytes accessed | tf_op | source)
XLA Modules:
  0.0 235.6 jit_solution(10482823808603668088)
XLA Ops:
  6.5 0.0 copy-start
  6.5 0.0 all-gather.3.cloned.1.call-start
  6.5 1.1 multiply_convert_fusion.2
  7.7 0.1 slice.264
  7.8 4.9 %collective-permute-start = (bf16[256,30]{1,0:T(8,128)(2,1)S(1)}, bf16[256,30]{1,0:T(8,128)(2,1)S(1)}, u32[]{:S(2)}, u32[]{:S(2)}) collective-permute-start(bf16[256,30]{1,0:T(8,128)(2,1)S(1)} %slice.264), channel_id=1, source_target_pairs={{0,4},{4,8},{8,12},{12,16},{16,20},{20,24},{24,28},{1,5},{5,9},{9,... | collective-permute-start | bytes 46088 | tf_op jit(solution)/shard_map/ppermute | solution.py:10
  12.6 1.0 fusion.55
  13.7 1.0 fusion.56
  14.7 0.8 copy.19
  15.5 0.1 eq.26
  15.6 0.1 reshape.110
  15.8 0.7 broadcast_multiply_fusion
  16.5 1.1 reduce-window.6
  17.6 0.2 slice_reduce_fusion
  17.9 0.1 fusion.42
  18.0 0.1 copy.23
  18.1 0.1 mul.489
  18.3 2.4 %scatter_custom_fusion.1 = s32[1024]{0:T(1024)S(1)} fusion(s32[512]{0:T(512)S(1)} %bitcast.67, s32[512]{0:T(512)S(1)} %add_select_fusion, s32[]{:T(128)} %constant.68.clone.1), kind=kCustom, calls=%fused_computation.104 | custom fusion | bytes 4100 | tf_op jit(solution)/shard_map/scatter | solution.py:62
  20.8 2.4 %scatter_custom_fusion = pred[1024]{0:T(1024)(128)(4,1)S(1)} fusion(s32[512]{0:T(512)S(1)} %bitcast.68, pred[512]{0:T(512)(128)(4,1)S(1)} %broadcast.118, pred[]{:T(512)} %constant.72.clone.1), kind=kCustom, calls=%fused_computation.107 | custom fusion | bytes 1025 | tf_op jit(solution)/shard_map/scatter | solution.py:63
  23.2 0.0 collective-permute-done
  23.2 0.1 maximum_convert_fusion
  23.4 0.0 copy-start.3
  23.4 0.0 copy-start.7
  23.4 3.5 %fusion.53 = (f32[256]{0:T(256)S(1)}, f32[256]{0:T(256)S(1)}, f32[256,256]{1,0:T(8,128)S(1)}) fusion(f32[256,286]{1,0:T(8,128)S(1)} %maximum_convert_fusion, f32[256]{0:T(256)S(1)} %bitcast.99, f32[256]{0:T(256)S(1)} %bitcast.100, f32[256]{0:T(256)S(1)} %bitcast.71, f32[256]{0:T(256)S(1)} %bitcast.72, f32[256]{0:T(256)S(1)} %bitcast.73, ...), kind=kLoop, calls=%fused_computation.114 | loop fusion | flops 4193792 | bytes 8422400 | tf_op jit(solution)/shard_map/reduce_sum | solution.py:41
  26.9 6.3 %all-reduce = (f32[256]{0:T(256)S(1)}, f32[256]{0:T(256)S(1)}) all-reduce(f32[256]{0:T(256)S(1)} %get-tuple-element.6, f32[256]{0:T(256)S(1)} %get-tuple-element.5), channel_id=1, replica_groups=mesh['sp'=8,'tp'=4] {'tp'}, use_global_device_ids=true, to_apply=%region_3.0 | all-reduce | flops 512 | bytes 4096 | tf_op jit(solution)/shard_map/psum | solution.py:40
  33.3 0.0 copy-done.3
  33.3 0.1 multiply_convert_fusion.1
  33.4 6.7 %all_gather.9 = bf16[1024,256]{1,0:T(8,128)(2,1)S(1)} all-gather(bf16[256,256]{1,0:T(8,128)(2,1)S(1)} %multiply_convert_fusion.1), channel_id=1, replica_groups=mesh['sp'=8,'tp'=4] {'tp'}, dimensions={0}, use_global_device_ids=true | all-gather | bytes 655360 | tf_op jit(solution)/shard_map/all_gather | solution.py:49
  40.2 0.0 copy-done
  40.2 0.0 copy-done.7
  40.2 0.5 fusion.11
  40.6 4.0 %gather_fusion = bf16[1024,512]{1,0:T(8,128)(2,1)S(1)} fusion(bf16[256,512]{1,0:T(8,128)(2,1)S(1)} %fusion.11, s32[1024]{0:T(1024)S(1)} %fusion.44), kind=kCustom, calls=%fused_computation | custom fusion | bytes 2101248 | tf_op jit(solution)/shard_map/jit(_take)/gather | solution.py:66
  44.6 0.5 select_select_fusion
  45.1 31.0 %all_to_all.10 = bf16[8,128,512]{2,1,0:T(8,128)(2,1)} all-to-all(bf16[8,128,512]{2,1,0:T(8,128)(2,1)S(1)} %select_select_fusion), channel_id=1, replica_groups=mesh['sp'=8,'tp'=4] {'sp'}, dimensions={0} | all-to-all | bytes 2097152 | tf_op jit(solution)/shard_map/all_to_all | solution.py:70
  76.1 0.0 all-gather.3.cloned.1.call-update
  76.1 0.2 all-gather.5.cloned.1.call-start
  76.4 32.9 %all-gather.3.cloned.1.call-done = bf16[8,128,2048]{2,1,0:T(8,128)(2,1)} async-done(((bf16[8,128,512]{2,1,0:T(8,128)(2,1)}), bf16[8,128,2048]{2,1,0:T(8,128)(2,1)}) %all-gather.3.cloned.1.call-update) | async-done | bytes 4194320 | tf_op jit(solution)/shard_map/all_gather | solution.py:69
  109.3 0.0 copy-start.5
  109.3 0.0 copy-start.6
  109.3 7.7 %fusion.2 = f32[1024,1024]{1,0:T(8,128)S(1)} fusion(bf16[1024,2048]{1,0:T(8,128)(2,1)} %bitcast.102, bf16[1,2048,1024]{2,1,0:T(8,128)(2,1)} %param.22), kind=kOutput, calls=%fused_computation.6 | convolution fusion | flops 4294967296 | bytes 12582912 | tf_op jit(solution)/shard_map/dot_general | solution.py:78
  116.9 0.0 copy-done.5
  116.9 0.0 copy-done.6
  116.9 6.4 %multiply_convert_fusion = bf16[1024,1024]{1,0:T(8,128)(2,1)} fusion(f32[1024,1024]{1,0:T(8,128)S(1)} %fusion.2, bf16[1024,2048]{1,0:T(8,128)(2,1)S(1)} %bitcast.103, bf16[1,2048,1024]{2,1,0:T(8,128)(2,1)S(1)} %copy-done.5), kind=kOutput, calls=%fused_computation.10 | convolution fusion | flops 4301258752 | bytes 14680064 | tf_op jit(solution)/shard_map/dot_general | solution.py:77
  123.3 0.0 all-gather.5.cloned.1.call-update
  123.3 0.0 copy-start.1
  123.4 0.0 copy-start.2
  123.4 0.0 copy-start.4
  123.4 58.4 %all-gather.5.cloned.1.call-done = bf16[1024,4096]{1,0:T(8,128)(2,1)} async-done(((bf16[1024,1024]{1,0:T(8,128)(2,1)}), bf16[1024,4096]{1,0:T(8,128)(2,1)}) %all-gather.5.cloned.1.call-update) | async-done | bytes 8388624 | tf_op jit(solution)/shard_map/all_gather | solution.py:82
  181.8 10.1 %fusion.8 = bf16[1024,512]{1,0:T(8,128)(2,1)} fusion(bf16[1024,4096]{1,0:T(8,128)(2,1)} %all-gather.5.cloned.1.call-done, bf16[1,4096,512]{2,1,0:T(8,128)(2,1)} %param.23), kind=kOutput, calls=%fused_computation.11 | convolution fusion | flops 4295491584 | bytes 13631488 | tf_op jit(solution)/shard_map/dot_general | solution.py:81
  191.9 5.5 %all-to-all-start.1 = ((bf16[8,128,512]{2,1,0:T(8,128)(2,1)}), bf16[8,128,512]{2,1,0:T(8,128)(2,1)S(1)}, u32[]{:S(2)}, u32[]{:S(2)}) async-start(bf16[8,128,512]{2,1,0:T(8,128)(2,1)} %bitcast.42), calls=%async_computation.1 | async-start | bytes 2097152 | tf_op jit(solution)/shard_map/all_to_all | solution.py:87
  197.4 0.1 sub.37
  197.5 0.1 copy.21
  197.6 0.0 copy-done.1
  197.6 0.2 copy.22
  197.8 0.0 copy-done.2
  197.9 0.0 copy-done.4
  197.9 0.1 copy.24
  198.1 25.5 %all-to-all-done.1 = bf16[8,128,512]{2,1,0:T(8,128)(2,1)S(1)} async-done(((bf16[8,128,512]{2,1,0:T(8,128)(2,1)}), bf16[8,128,512]{2,1,0:T(8,128)(2,1)S(1)}, u32[]{:S(2)}, u32[]{:S(2)}) %all-to-all-start.1) | async-done | bytes 1048608 | tf_op jit(solution)/shard_map/all_to_all | solution.py:87
  223.6 2.0 gather_fusion.1
  225.6 0.2 gather.15
  225.8 2.2 multiply_reduce_fusion
  228.0 0.8 add_convert_fusion
  (15 shorter events, 0.2 us)
Async XLA Ops:
  6.5 33.6 %copy-start = (bf16[1024,512]{1,0:T(8,128)(2,1)S(1)}, bf16[1024,512]{1,0:T(8,128)(2,1)}, u32[]{:S(2)}) copy-start(bf16[1024,512]{1,0:T(8,128)(2,1)} %param.16) | copy-start | bytes 3145732
  6.5 102.7 %all-gather.3.cloned.1.call-start = ((), (), s32[]{:S(2)}) async-start(), calls=%async_computation.2 | async-start | bytes 5242880 | tf_op jit(solution)/shard_map/all_gather | solution.py:69
  7.8 15.5 %collective-permute-start = (bf16[256,30]{1,0:T(8,128)(2,1)S(1)}, bf16[256,30]{1,0:T(8,128)(2,1)S(1)}, u32[]{:S(2)}, u32[]{:S(2)}) collective-permute-start(bf16[256,30]{1,0:T(8,128)(2,1)S(1)} %slice.264), channel_id=1, source_target_pairs={{0,4},{4,8},{8,12},{12,16},{16,20},{20,24},{24,28},{1,5},{5,9},{9,... | collective-permute-start | bytes 46088 | tf_op jit(solution)/shard_map/ppermute | solution.py:10
  23.4 9.9 %copy-start.3 = (f32[256]{0:T(256)S(1)}, f32[256]{0:T(256)}, u32[]{:S(2)}) copy-start(f32[256]{0:T(256)} %param.15) | copy-start | bytes 3076
  23.4 16.8 %copy-start.7 = (bf16[256,512]{1,0:T(8,128)(2,1)S(1)}, bf16[256,512]{1,0:T(8,128)(2,1)}, u32[]{:S(2)}) copy-start(bf16[256,512]{1,0:T(8,128)(2,1)} %param.17) | copy-start | bytes 786436
  76.1 105.6 %all-gather.5.cloned.1.call-start = ((), (), s32[]{:S(2)}) async-start(), calls=%async_computation.3 | async-start | bytes 10485760 | tf_op jit(solution)/shard_map/all_gather | solution.py:82
  109.3 7.7 %copy-start.5 = (bf16[1,2048,1024]{2,1,0:T(8,128)(2,1)S(1)}, bf16[1,2048,1024]{2,1,0:T(8,128)(2,1)}, u32[]{:S(2)}) copy-start(bf16[1,2048,1024]{2,1,0:T(8,128)(2,1)} %param.21) | copy-start | bytes 12582916
  109.3 7.7 %copy-start.6 = (bf16[8,128,2048]{2,1,0:T(8,128)(2,1)S(1)}, bf16[8,128,2048]{2,1,0:T(8,128)(2,1)}, u32[]{:S(2)}) copy-start(bf16[8,128,2048]{2,1,0:T(8,128)(2,1)} %all-gather.3.cloned.1.call-done) | copy-start | bytes 12582916
  123.3 74.3 %copy-start.1 = (s32[256,2]{0,1:T(2,128)S(1)}, s32[256,2]{0,1:T(2,128)}, u32[]{:S(2)}) copy-start(s32[256,2]{0,1:T(2,128)} %param.18) | copy-start | bytes 6148
  123.4 74.5 %copy-start.2 = (f32[256,2]{0,1:T(2,128)S(1)}, f32[256,2]{0,1:T(2,128)}, u32[]{:S(2)}) copy-start(f32[256,2]{0,1:T(2,128)} %param.19) | copy-start | bytes 6148
  123.4 74.5 %copy-start.4 = (f32[256]{0:T(256)S(1)}, f32[256]{0:T(256)}, u32[]{:S(2)}) copy-start(f32[256]{0:T(256)} %param.20) | copy-start | bytes 3076
  191.9 31.7 %all-to-all-start.1 = ((bf16[8,128,512]{2,1,0:T(8,128)(2,1)}), bf16[8,128,512]{2,1,0:T(8,128)(2,1)S(1)}, u32[]{:S(2)}, u32[]{:S(2)}) async-start(bf16[8,128,512]{2,1,0:T(8,128)(2,1)} %bitcast.42), calls=%async_computation.1 | async-start | bytes 2097152 | tf_op jit(solution)/shard_map/all_to_all | solution.py:87
Sparse Core Ops, SparseCore 0:
  76.2 32.9 all-gather.2
  123.5 58.2 all-gather.4
where the time goes:
time: 236 us
  waiting for transfers between devices  117 us (50%)
  blocking collectives  44.1 us (19%)
  matrix products  24.6 us (10%)
  local copies, waits for them, and re-layouts  15.3 us (6%)
  between operations  13.7 us (6%)
  starting transfers between devices  10.6 us (4%)
  other arithmetic  10.4 us (4%)
    all_gather x1, waiting for transfers between devices, per_device(): lax.all_gather(hidden, 'tp', axis=1, tiled=True)  58.4 us
    all_gather x1, waiting for transfers between devices, per_device(): lax.all_gather(lax.all_to_all(outgoing, 'sp', split_axis=0, concat_axis=0...  32.9 us
    all_to_all x1, blocking collectives, per_device(): lax.all_to_all(outgoing, 'sp', split_axis=0, concat_axis=0, tiled=True)  31 us
    all_to_all x1, waiting for transfers between devices, per_device(): lax.all_to_all(results, 'sp', split_axis=0, concat_axis=0, tiled=True)  25.5 us
    dot_general x1, matrix products, per_device(): jnp.dot(lax.all_gather(hidden, 'tp', axis=1, tiled=True), weights, prefer...  10.1 us
    dot_general x1, matrix products, per_device(): up_part = jnp.dot(flat_rows, w_up[0], preferred_element_type=jnp.float32)  7.65 us
    all_gather x1, blocking collectives, per_device(): lax.all_gather(activated, 'tp', axis=0, tiled=True)  6.74 us
    dot_general x1, matrix products, per_device(): jnp.dot(flat_rows, w_gate[0], preferred_element_type=jnp.float32)  6.37 us
  transfers between devices with their start and end apart: 4, of which 3 were waited for; matrix products, arithmetic and copies ran while one was open for 5% of the time, Pallas kernels for 0%

commit v1 on v0

--- a/solution.py
+++ b/solution.py
@@ -1,7 +1,264 @@
+import functools
+
 import jax
 import jax.numpy as jnp
 from jax import lax
+from jax.experimental import pallas as pl
+from jax.experimental.pallas import tpu as pltpu
 from jax.sharding import PartitionSpec as P
+
+MESH = pl.DeviceIdType.MESH
+
+
+def expert_kernel(
+    n_sp,
+    n_tp,
+    outgoing,
+    w_gate,
+    w_up,
+    w_down,
+    returned,
+    rows,
+    hidden,
+    results,
+    gate_v,
+    up_v,
+    down_v,
+    load_sem,
+    own_sem,
+    out_send,
+    rows_recv,
+    rows_far,
+    rows_near,
+    hid_recv,
+    hid_far,
+    hid_near,
+    ret_send,
+    ret_recv,
+):
+    e = lax.axis_index("sp")
+    q = lax.axis_index("tp")
+    n_y = n_tp // 2
+    y, core = q // 2, q % 2
+    sibling = 2 * y + (1 - core)
+    width = outgoing.shape[2]
+    ff_local = gate_v.shape[1]
+
+    def source(k):
+        return lax.rem(e + k, n_sp)
+
+    def rows_at(s, t):
+        return rows.at[s, :, pl.ds(pl.multiple_of(t * width, width), width)]
+
+    def hidden_at(s, t):
+        return hidden.at[s, :, pl.ds(pl.multiple_of(t * ff_local, ff_local), ff_local)]
+
+    def far(j):
+        return 2 * lax.rem(y + j, n_y) + core
+
+    def behind(j):
+        return 2 * lax.rem(y + n_y - j, n_y) + core
+
+    def share(at, recv, s, t, send, peer):
+        return pltpu.make_async_remote_copy(
+            src_ref=at(s, t),
+            dst_ref=at(s, t),
+            send_sem=send,
+            recv_sem=recv.at[s, t],
+            device_id=(e, peer),
+            device_id_type=MESH,
+        )
+
+    def dispatch(k):
+        to = lax.rem(e + n_sp - k, n_sp)
+        return pltpu.make_async_remote_copy(
+            src_ref=outgoing.at[to],
+            dst_ref=rows_at(e, q),
+            send_sem=out_send.at[k],
+            recv_sem=rows_recv.at[e, q],
+            device_id=(to, q),
+            device_id_type=MESH,
+        )
+
+    def give_back(k):
+        s = source(k)
+        return pltpu.make_async_remote_copy(
+            src_ref=results.at[s],
+            dst_ref=returned.at[e],
+            send_sem=ret_send.at[k],
+            recv_sem=ret_recv.at[e],
+            device_id=(s, q),
+            device_id_type=MESH,
+        )
+
+    def arrived(at, recv, s, t):
+        pltpu.make_async_copy(at(s, t), at(s, t), recv.at[s, t]).wait()
+
+    loads = [
+        pltpu.make_async_copy(w_gate.at[0], gate_v, load_sem.at[0]),
+        pltpu.make_async_copy(w_up.at[0], up_v, load_sem.at[1]),
+        pltpu.make_async_copy(w_down.at[0], down_v, load_sem.at[2]),
+    ]
+    own_in = pltpu.make_async_copy(outgoing.at[e], rows_at(e, q), own_sem.at[0])
+    own_in.start()
+
+    barrier = pltpu.get_barrier_semaphore()
+
+    @pl.loop(1, n_sp)
+    def _(k):
+        pl.semaphore_signal(barrier, inc=1, device_id=(source(k), q), device_id_type=MESH)
+
+    for j in range(1, n_y):
+        pl.semaphore_signal(barrier, inc=1, device_id=(e, far(j)), device_id_type=MESH)
+    pl.semaphore_signal(barrier, inc=1, device_id=(e, sibling), device_id_type=MESH)
+    pl.semaphore_wait(barrier, n_sp - 1 + n_y)
+
+    @pl.loop(1, n_sp)
+    def _(k):
+        dispatch(k).start()
+
+    for load in loads:
+        load.start()
+
+    def spread(at, recv, far_sem, near_sem, s):
+        for j in range(1, n_y):
+            share(at, recv, s, q, far_sem.at[s, j], far(j)).start()
+        share(at, recv, s, q, near_sem.at[s, 0], sibling).start()
+
+    def relay(at, recv, near_sem, s):
+        for j in range(1, n_y):
+            t = behind(j)
+            arrived(at, recv, s, t)
+            share(at, recv, s, t, near_sem.at[s, j], sibling).start()
+
+    def collect(at, recv, s):
+        for j in range(n_y):
+            arrived(at, recv, s, 2 * lax.rem(y + n_y - j, n_y) + (1 - core))
+
+    def drain(at, recv, far_sem, near_sem, s):
+        for j in range(1, n_y):
+            share(at, recv, s, q, far_sem.at[s, j], far(j)).wait_send()
+        share(at, recv, s, q, near_sem.at[s, 0], sibling).wait_send()
+        for j in range(1, n_y):
+            share(at, recv, s, behind(j), near_sem.at[s, j], sibling).wait_send()
+
+    tile = min(256, ff_local)
+    out_tile = min(256, width)
+
+    def up_step(s):
+        @pl.loop(0, ff_local // tile)
+        def _(i):
+            at = pl.ds(pl.multiple_of(i * tile, tile), tile)
+            g = jnp.dot(rows[s], gate_v[:, at], preferred_element_type=jnp.float32)
+            u = jnp.dot(rows[s], up_v[:, at], preferred_element_type=jnp.float32)
+            h = (g / (1.0 + jnp.exp(-g)) * u).astype(hidden.dtype)
+            hidden[s, :, pl.ds(pl.multiple_of(q * ff_local + i * tile, tile), tile)] = h
+
+    def down_step(s):
+        @pl.loop(0, width // out_tile)
+        def _(i):
+            at = pl.ds(pl.multiple_of(i * out_tile, out_tile), out_tile)
+            o = jnp.dot(hidden[s], down_v[:, at], preferred_element_type=jnp.float32)
+            results[s, :, at] = o.astype(results.dtype)
+
+    @pl.loop(0, n_sp + 4)
+    def _(i):
+        @pl.when(i < n_sp)
+        def _():
+            @pl.when(i == 0)
+            def _():
+                own_in.wait()
+
+            @pl.when(i > 0)
+            def _():
+                arrived(rows_at, rows_recv, source(i), q)
+
+            spread(rows_at, rows_recv, rows_far, rows_near, source(i))
+
+        @pl.when((i >= 1) & (i < n_sp + 1))
+        def _():
+            relay(rows_at, rows_recv, rows_near, source(i - 1))
+
+        @pl.when((i >= 2) & (i < n_sp + 2))
+        def _():
+            s = source(i - 2)
+            collect(rows_at, rows_recv, s)
+
+            @pl.when(i == 2)
+            def _():
+                for load in loads:
+                    load.wait()
+
+            up_step(s)
+            spread(hidden_at, hid_recv, hid_far, hid_near, s)
+
+        @pl.when((i >= 3) & (i < n_sp + 3))
+        def _():
+            relay(hidden_at, hid_recv, hid_near, source(i - 3))
+
+        @pl.when(i >= 4)
+        def _():
+            s = source(i - 4)
+            collect(hidden_at, hid_recv, s)
+            down_step(s)
+
+            @pl.when(i == 4)
+            def _():
+                pltpu.make_async_copy(results.at[e], returned.at[e], own_sem.at[1]).start()
+
+            @pl.when(i > 4)
+            def _():
+                give_back(i - 4).start()
+
+    pltpu.make_async_copy(results.at[e], returned.at[e], own_sem.at[1]).wait()
+
+    @pl.loop(0, n_sp)
+    def _(s):
+        drain(rows_at, rows_recv, rows_far, rows_near, s)
+        drain(hidden_at, hid_recv, hid_far, hid_near, s)
+
+    @pl.loop(1, n_sp)
+    def _(k):
+        dispatch(k).wait_send()
+        give_back(k).wait_send()
+        s = source(k)
+        pltpu.make_async_copy(returned.at[s], returned.at[s], ret_recv.at[s]).wait()
+
+
+def run_experts(outgoing, w_gate, w_up, w_down):
+    n_sp, n_tp = lax.axis_size("sp"), lax.axis_size("tp")
+    n_y = n_tp // 2
+    _, capacity, width = outgoing.shape
+    ff_local = w_gate.shape[2]
+    dma = pltpu.SemaphoreType.DMA
+    return pl.pallas_call(
+        functools.partial(expert_kernel, n_sp, n_tp),
+        out_shape=jax.ShapeDtypeStruct(outgoing.shape, outgoing.dtype),
+        in_specs=[pl.BlockSpec(memory_space=pl.ANY)] * 4,
+        out_specs=pl.BlockSpec(memory_space=pl.ANY),
+        scratch_shapes=[
+            pltpu.VMEM((n_sp, capacity, width * n_tp), jnp.bfloat16),
+            pltpu.VMEM((n_sp, capacity, ff_local * n_tp), jnp.bfloat16),
+            pltpu.VMEM(outgoing.shape, jnp.bfloat16),
+            pltpu.VMEM(w_gate.shape[1:], jnp.bfloat16),
+            pltpu.VMEM(w_up.shape[1:], jnp.bfloat16),
+            pltpu.VMEM(w_down.shape[1:], jnp.bfloat16),
+            dma((3,)),
+            dma((2,)),
+            dma((n_sp,)),
+            dma((n_sp, n_tp)),
+            dma((n_sp, n_y)),
+            dma((n_sp, n_y)),
+            dma((n_sp, n_tp)),
+            dma((n_sp, n_y)),
+            dma((n_sp, n_y)),
+            dma((n_sp,)),
+            dma((n_sp,)),
+        ],
+        compiler_params=pltpu.CompilerParams(
+            collective_id=0, has_side_effects=True, vmem_limit_bytes=48 * 1024 * 1024
+        ),
+    )(outgoing, w_gate, w_up, w_down)
 
 
 def from_behind(block, axis, distance):
@@ -60,31 +317,9 @@
     slot = flat_ids * capacity + rank
     token_of = jnp.arange(flat_ids.shape[0], dtype=jnp.int32) // expert_ids.shape[1]
     table = jnp.zeros((experts * capacity,), jnp.int32).at[slot].set(token_of)
-    filled = jnp.zeros((experts * capacity,), jnp.bool_).at[slot].set(True)
     route_weight = (group_prob[:, None] * jax.nn.softmax(route_logits, axis=-1)).reshape(-1)
-    outgoing = jnp.where(
-        filled[:, None], jnp.take(mixed, table, axis=0), jnp.zeros((), jnp.bfloat16)
-    )
-    outgoing = outgoing.reshape(experts, capacity, mixed.shape[1])
-    rows = lax.all_gather(
-        lax.all_to_all(outgoing, "sp", split_axis=0, concat_axis=0, tiled=True),
-        "tp",
-        axis=2,
-        tiled=True,
-    )
-    sources, count, width = rows.shape
-    flat_rows = rows.reshape(sources * count, width)
-    gate_part = jnp.dot(flat_rows, w_gate[0], preferred_element_type=jnp.float32)
-    up_part = jnp.dot(flat_rows, w_up[0], preferred_element_type=jnp.float32)
-    hidden = (jax.nn.silu(gate_part) * up_part).astype(jnp.bfloat16)
-    weights = w_down[0]
-    expert_out = jnp.dot(
-        lax.all_gather(hidden, "tp", axis=1, tiled=True),
-        weights,
-        preferred_element_type=jnp.float32,
-    )
-    results = expert_out.astype(jnp.bfloat16).reshape(sources, count, w_down.shape[2])
-    returned = lax.all_to_all(results, "sp", split_axis=0, concat_axis=0, tiled=True)
+    outgoing = jnp.take(mixed, table, axis=0).reshape(experts, capacity, mixed.shape[1])
+    returned = run_experts(outgoing, w_gate, w_up, w_down)
     flat_back = returned.reshape(experts * capacity, returned.shape[2])
     picked = jnp.take(flat_back, slot, axis=0).astype(jnp.float32) * route_weight[:, None]
     routed = jnp.sum(picked.reshape(local_tokens, expert_ids.shape[1], flat_back.shape[1]), axis=1)

time: 236 us -> 134 us (0.57)
  waiting for transfers between devices: 117 us -> 0.01 us
  Pallas kernels: 0 us -> 89.1 us
  blocking collectives: 44.1 us -> 13.1 us
  matrix products: 24.6 us -> 0.45 us
  between operations: 13.7 us -> 0.22 us
  starting transfers between devices: 10.6 us -> 4.87 us
  other arithmetic: 10.4 us -> 12.9 us
  local copies, waits for them, and re-layouts: 15.3 us -> 12.8 us
    all_gather x2 -> x0, waiting for transfers between devices: 91.3 us -> none  [the longest x1 58.4 us: per_device(): lax.all_gather(hidden, 'tp', axis=1, tiled=True)]
    pallas_call x0 -> x1, Pallas kernels: none -> 89.1 us  [run_experts(): pl.pallas_call(functools.partial(expert_kernel, n_sp, n_tp), out_shape=ja...]
    all_to_all x1 -> x0, blocking collectives: 31 us -> none  [per_device(): lax.all_to_all(outgoing, 'sp', split_axis=0, concat_axis=0, tiled=True)]
    all_to_all x1 -> x0, waiting for transfers between devices: 25.5 us -> none  [per_device(): lax.all_to_all(results, 'sp', split_axis=0, concat_axis=0, tiled=True)]
    dot_general x3 -> x0, matrix products: 24.2 us -> none  [the longest x1 10.1 us: per_device(): jnp.dot(lax.all_gather(hidden, 'tp', axis=1, tiled=True), weights, prefer...]
    all_to_all x1 -> x0, starting transfers between devices: 5.5 us -> none  [per_device(): lax.all_to_all(results, 'sp', split_axis=0, concat_axis=0, tiled=True)]
    scatter x1 -> x0, local copies, waits for them, and re-layouts: 2.45 us -> none  [per_device(): filled = jnp.zeros((experts * capacity,), jnp.bool_).at[slot].set(True)]
  transfers between devices with their start and end apart: 4 -> 1, of which waited for: 3 -> 0; matrix products, arithmetic and copies ran while one was open for 5% -> 9% of each run, Pallas kernels for 0% -> 0%
where the time goes in v1:
time: 134 us; the launch traced here: 133 us
  Pallas kernels  89.1 us (66%)
  blocking collectives  13.1 us (10%)
  other arithmetic  12.9 us (10%)
  local copies, waits for them, and re-layouts  12.8 us (10%)
  starting transfers between devices  4.87 us (4%)
    pallas_call x1, Pallas kernels, run_experts(): pl.pallas_call(functools.partial(expert_kernel, n_sp, n_tp), out_shape=ja...  89.1 us
    all_gather x1, blocking collectives, per_device(): lax.all_gather(activated, 'tp', axis=0, tiled=True)  6.74 us
    psum x1, blocking collectives, per_device(): lax.psum((jnp.sum(filtered, axis=0), jnp.sum(filtered * filtered, axis=0)...  6.33 us
    ppermute x1, starting transfers between devices, from_behind(): return lax.ppermute(block, axis, route)  4.87 us
    gather x1, local copies, waits for them, and re-layouts, per_device(): jnp.take(mixed, table, axis=0).reshape(experts, capacity, mixed.shape[1])  3.97 us
    reduce_sum x1, other arithmetic, per_device(): jnp.sum(filtered, axis=0)  3.54 us
  transfers between devices with their start and end apart: 1, of which 0 were waited for; matrix products, arithmetic and copies ran while one was open for 9% of the time, Pallas kernels for 0%

profile of v1, /device:TPU:0, one launch (start us, length us, event | category | flops | bytes accessed | tf_op | source)
XLA Modules:
  0.0 133.4 jit_solution(3044588436352681263)
XLA Ops:
  0.0 0.0 copy-start
  0.0 1.1 multiply_convert_fusion.1
  1.1 0.1 slice.264
  1.2 4.9 %collective-permute-start = (bf16[256,30]{1,0:T(8,128)(2,1)S(1)}, bf16[256,30]{1,0:T(8,128)(2,1)S(1)}, u32[]{:S(2)}, u32[]{:S(2)}) collective-permute-start(bf16[256,30]{1,0:T(8,128)(2,1)S(1)} %slice.264), channel_id=1, source_target_pairs={{0,4},{4,8},{8,12},{12,16},{16,20},{20,24},{24,28},{1,5},{5,9},{9,... | collective-permute-start | bytes 46088 | tf_op jit(solution)/shard_map/ppermute | solution.py:267
  6.1 1.0 fusion.42
  7.1 1.0 fusion.43
  8.1 0.8 copy.19
  8.9 0.1 eq.26
  9.1 0.1 reshape.98
  9.2 0.7 broadcast_multiply_fusion
  9.9 1.1 reduce-window.6
  11.1 0.2 slice_reduce_fusion
  11.3 0.1 fusion.31
  11.4 0.1 copy.23
  11.6 0.1 mul.482
  11.7 2.4 %scatter_custom_fusion = s32[1024]{0:T(1024)S(1)} fusion(s32[512]{0:T(512)S(1)} %bitcast.48, s32[512]{0:T(512)S(1)} %add_select_fusion, s32[]{:T(128)} %constant.63.clone.1), kind=kCustom, calls=%fused_computation.95 | custom fusion | bytes 4100 | tf_op jit(solution)/shard_map/scatter | solution.py:319
  14.2 0.1 sub.37
  14.4 0.1 copy.21
  14.4 0.7 compare_and_fusion
  15.1 0.7 reduce_max.9
  15.8 0.7 fusion.39
  16.5 0.7 divide_multiply_fusion
  17.3 0.2 copy.22
  17.4 0.1 copy.24
  17.6 0.0 collective-permute-done
  17.6 0.1 maximum_convert_fusion
  17.7 0.0 copy-start.1
  17.7 0.0 copy-start.2
  17.8 3.5 %fusion.40 = (f32[256]{0:T(256)S(1)}, f32[256]{0:T(256)S(1)}, f32[256,256]{1,0:T(8,128)S(1)}) fusion(f32[256,286]{1,0:T(8,128)S(1)} %maximum_convert_fusion, f32[256]{0:T(256)S(1)} %bitcast.79, f32[256]{0:T(256)S(1)} %bitcast.80, f32[256]{0:T(256)S(1)} %bitcast.51, f32[256]{0:T(256)S(1)} %bitcast.52, f32[256]{0:T(256)S(1)} %bitcast.53, f32[256]{0:T(256)S(1)} %bitcast.54, ...), kind=kLoop, calls=%fused_computation.103 | loop fusion | flops 4193792 | bytes 8422400 | tf_op jit(solution)/shard_map/reduce_sum | solution.py:298
  21.3 6.3 %all-reduce = (f32[256]{0:T(256)S(1)}, f32[256]{0:T(256)S(1)}) all-reduce(f32[256]{0:T(256)S(1)} %get-tuple-element.6, f32[256]{0:T(256)S(1)} %get-tuple-element.5), channel_id=1, replica_groups=mesh['sp'=8,'tp'=4] {'tp'}, use_global_device_ids=true, to_apply=%region_3.0 | all-reduce | flops 512 | bytes 4096 | tf_op jit(solution)/shard_map/psum | solution.py:297
  27.6 0.0 copy-done.1
  27.6 0.1 multiply_convert_fusion
  27.8 6.7 %all_gather.3 = bf16[1024,256]{1,0:T(8,128)(2,1)S(1)} all-gather(bf16[256,256]{1,0:T(8,128)(2,1)S(1)} %multiply_convert_fusion), channel_id=1, replica_groups=mesh['sp'=8,'tp'=4] {'tp'}, dimensions={0}, use_global_device_ids=true | all-gather | bytes 655360 | tf_op jit(solution)/shard_map/all_gather | solution.py:306
  34.5 0.0 copy-done
  34.5 0.0 copy-done.2
  34.6 0.5 fusion
  35.0 4.0 %gather_fusion = bf16[1024,512]{1,0:T(8,128)(2,1)S(1)} fusion(bf16[256,512]{1,0:T(8,128)(2,1)S(1)} %fusion, s32[1024]{0:T(1024)S(1)} %fusion.33), kind=kCustom, calls=%fused_computation | custom fusion | bytes 2101248 | tf_op jit(solution)/shard_map/jit(_take)/gather | solution.py:321
  39.0 0.2 broadcast_select_fusion.outgoing
  39.2 89.1 %shard_map.118 = bf16[8,128,512]{2,1,0:T(8,128)(2,1)S(1)} custom-call(bf16[8,128,512]{2,1,0:T(8,128)(2,1)S(1)} %broadcast_select_fusion.outgoing, bf16[1,2048,1024]{2,1,0:T(8,128)(2,1)} %w_gate.1, bf16[1,2048,1024]{2,1,0:T(8,128)(2,1)} %w_up.1, bf16[1,4096,512]{2,1,0:T(8,128)(2,1)} %w_down.1), custom_call_target="tpu_custom_call" | custom-call | tf_op jit(solution)/shard_map/pallas_call | solution.py:234
  128.3 2.0 %gather_fusion.1 = bf16[512,512]{1,0:T(8,128)(2,1)S(1)} fusion(bf16[1024,512]{1,0:T(8,128)(2,1)S(1)} %bitcast.45, s32[1024]{0:T(1024)S(1)} %pad_clamp_fusion), kind=kCustom, calls=%fused_computation.1 | custom fusion | bytes 1050624 | tf_op jit(solution)/shard_map/jit(_take)/gather | solution.py:324
  130.2 0.2 gather.15
  130.4 2.2 %multiply_reduce_fusion = f32[256,512]{1,0:T(8,128)S(1)} fusion(bf16[256,2,512]{2,1,0:T(2,128)(2,1)S(1)} %gather.15, pred[256,2]{1,0:T(8,128)(4,1)S(1)} %copy.22, f32[256,2]{1,0:T(8,128)S(1)} %copy.24), kind=kLoop, calls=%fused_computation.5 | loop fusion | flops 917504 | bytes 1051136 | tf_op jit(solution)/shard_map/reduce_sum | solution.py:325
  132.6 0.8 add_convert_fusion
  (10 shorter events, 0.1 us)
Async XLA Ops:
  0.0 34.5 %copy-start = (bf16[1024,512]{1,0:T(8,128)(2,1)S(1)}, bf16[1024,512]{1,0:T(8,128)(2,1)}, u32[]{:S(2)}) copy-start(bf16[1024,512]{1,0:T(8,128)(2,1)} %param.16) | copy-start | bytes 3145732
  1.2 16.4 %collective-permute-start = (bf16[256,30]{1,0:T(8,128)(2,1)S(1)}, bf16[256,30]{1,0:T(8,128)(2,1)S(1)}, u32[]{:S(2)}, u32[]{:S(2)}) collective-permute-start(bf16[256,30]{1,0:T(8,128)(2,1)S(1)} %slice.264), channel_id=1, source_target_pairs={{0,4},{4,8},{8,12},{12,16},{16,20},{20,24},{24,28},{1,5},{5,9},{9,... | collective-permute-start | bytes 46088 | tf_op jit(solution)/shard_map/ppermute | solution.py:267
  17.7 9.9 %copy-start.1 = (f32[256]{0:T(256)S(1)}, f32[256]{0:T(256)}, u32[]{:S(2)}) copy-start(f32[256]{0:T(256)} %param.15) | copy-start | bytes 3076
  17.7 16.8 %copy-start.2 = (bf16[256,512]{1,0:T(8,128)(2,1)S(1)}, bf16[256,512]{1,0:T(8,128)(2,1)}, u32[]{:S(2)}) copy-start(bf16[256,512]{1,0:T(8,128)(2,1)} %param.17) | copy-start | bytes 786436

commit v2 on v1

v2 whole, which is shorter than its diff:
```python
import functools

import jax
import jax.numpy as jnp
from jax import lax
from jax.experimental import pallas as pl
from jax.experimental.pallas import tpu as pltpu
from jax.sharding import PartitionSpec as P

MESH = pl.DeviceIdType.MESH


def expert_kernel(
    n_sp,
    n_tp,
    filtered,
    gain,
    proj,
    resid,
    slot_rows,
    slot_cols,
    route,
    w_gate,
    w_up,
    w_down,
    out,
    stats,
    act,
    mixed,
    total,
    outgoing,
    rows,
    hidden,
    results,
    returned,
    gate_v,
    up_v,
    down_v,
    load_sem,
    own_sem,
    stat_send,
    stat_recv,
    act_recv,
    act_far,
    act_near,
    mix_send,
    mix_recv,
    out_send,
    rows_recv,
    rows_near,
    hid_recv,
    hid_far,
    hid_near,
    ret_send,
    ret_recv,
):
    e = lax.axis_index("sp")
    q = lax.axis_index("tp")
    n_y = n_tp // 2
    y, core = q // 2, q % 2
    sibling = 2 * y + (1 - core)
    _, capacity, width = results.shape
    wide = n_y * width
    tokens = mixed.shape[0]
    ff_local = gate_v.shape[1]

    def source(k):
        return lax.rem(e + k, n_sp)

    def rows_at(s, c):
        return rows.at[s, :, pl.ds(pl.multiple_of(c * wide, wide), wide)]

    def act_at(s, t):
        return act.at[t]

    def mixed_at(t):
        return mixed.at[:, pl.ds(pl.multiple_of((t // 2) * width, width), width)]

    def hidden_at(s, t):
        return hidden.at[s, :, pl.ds(pl.multiple_of(t * ff_local, ff_local), ff_local)]

    def far(j):
        return 2 * lax.rem(y + j, n_y) + core

    def behind(j):
        return 2 * lax.rem(y + n_y - j, n_y) + core

    def share(at, recv, s, t, send, peer):
        return pltpu.make_async_remote_copy(
            src_ref=at(s, t),
            dst_ref=at(s, t),
            send_sem=send,
            recv_sem=recv.at[s, t],
            device_id=(e, peer),
            device_id_type=MESH,
        )

    def dispatch(k):
        to = lax.rem(e + n_sp - k, n_sp)
        return pltpu.make_async_remote_copy(
            src_ref=outgoing.at[to],
            dst_ref=rows_at(e, core),
            send_sem=out_send.at[k],
            recv_sem=rows_recv.at[e, core],
            device_id=(to, q),
            device_id_type=MESH,
        )

    def give_back(k):
        s = source(k)
        return pltpu.make_async_remote_copy(
            src_ref=results.at[s],
            dst_ref=returned.at[e],
            send_sem=ret_send.at[k],
            recv_sem=ret_recv.at[e],
            device_id=(s, q),
            device_id_type=MESH,
        )

    def arrived(at, recv, s, t):
        pltpu.make_async_copy(at(s, t), at(s, t), recv.at[s, t]).wait()

    def tell(o):
        return pltpu.make_async_remote_copy(
            src_ref=stats.at[q],
            dst_ref=stats.at[q],
            send_sem=stat_send.at[o],
            recv_sem=stat_recv.at[q],
            device_id=(e, lax.rem(q + o, n_tp)),
            device_id_type=MESH,
        )

    def cross(j):
        return pltpu.make_async_remote_copy(
            src_ref=mixed_at(q),
            dst_ref=mixed_at(q),
            send_sem=mix_send.at[j],
            recv_sem=mix_recv.at[y],
            device_id=(e, far(j)),
            device_id_type=MESH,
        )

    loads = [pltpu.make_async_copy(w_down.at[0], down_v, load_sem.at[2, 0])]
    for t in range(n_tp):
        to = pl.ds((t % 2 * n_y + t // 2) * width, width)
        at = pl.ds(t * width, width)
        loads.append(pltpu.make_async_copy(w_gate.at[0, at], gate_v.at[to], load_sem.at[0, t]))
        loads.append(pltpu.make_async_copy(w_up.at[0, at], up_v.at[to], load_sem.at[1, t]))

    barrier = pltpu.get_barrier_semaphore()

    @pl.loop(1, n_sp)
    def _(k):
        pl.semaphore_signal(barrier, inc=1, device_id=(source(k), q), device_id_type=MESH)

    for o in range(1, n_tp):
        pl.semaphore_signal(
            barrier, inc=1, device_id=(e, lax.rem(q + o, n_tp)), device_id_type=MESH
        )
    for load in loads:
        load.start()

    raw = filtered[...]
    stats[q, 0:1] = jnp.sum(raw, axis=0, keepdims=True)
    stats[q, 1:2] = jnp.sum(raw * raw, axis=0, keepdims=True)
    pl.semaphore_wait(barrier, n_sp - 1 + n_tp - 1)

    def spread(at, recv, far_sem, near_sem, s):
        for j in range(1, n_y):
            share(at, recv, s, q, far_sem.at[s, j], far(j)).start()
        share(at, recv, s, q, near_sem.at[s, 0], sibling).start()

    def relay(at, recv, near_sem, s):
        for j in range(1, n_y):
            t = behind(j)
            arrived(at, recv, s, t)
            share(at, recv, s, t, near_sem.at[s, j], sibling).start()

    def collect(at, recv, s):
        for j in range(n_y):
            arrived(at, recv, s, 2 * lax.rem(y + n_y - j, n_y) + (1 - core))

    def drain(at, recv, far_sem, near_sem, s):
        for j in range(1, n_y):
            share(at, recv, s, q, far_sem.at[s, j], far(j)).wait_send()
        share(at, recv, s, q, near_sem.at[s, 0], sibling).wait_send()
        for j in range(1, n_y):
            share(at, recv, s, behind(j), near_sem.at[s, j], sibling).wait_send()

    for o in range(1, n_tp):
        tell(o).start()
    for o in range(1, n_tp):
        t = lax.rem(q + o, n_tp)
        pltpu.make_async_copy(stats.at[t], stats.at[t], stat_recv.at[t]).wait()
    one = stats[0, 0:1]
    two = stats[0, 1:2]
    for t in range(1, n_tp):
        one = one + stats[t, 0:1]
        two = two + stats[t, 1:2]
    channels = proj.shape[0]
    mean = one / channels
    var = two / channels - mean * mean
    normed = (filtered[...] - mean) * lax.rsqrt(var + 1e-05) * gain[...]
    act[q] = (normed / (1.0 + jnp.exp(-normed))).astype(act.dtype)
    spread(act_at, act_recv, act_far, act_near, 0)
    relay(act_at, act_recv, act_near, 0)
    collect(act_at, act_recv, 0)
    depth = act.shape[1]
    sums = resid[...].astype(jnp.float32)
    for t in range(n_tp):
        sums = sums + lax.dot_general(
            act[t],
            proj[t * depth : (t + 1) * depth],
            (((0,), (0,)), ((), ())),
            preferred_element_type=jnp.float32,
        )
    own_columns = pl.ds(pl.multiple_of(y * width, width), width)
    mixed[:, own_columns] = sums.astype(mixed.dtype)
    for j in range(1, n_y):
        cross(j).start()
    total[...] = jnp.zeros_like(total)
    for j in range(1, n_y):
        t = behind(j)
        pltpu.make_async_copy(mixed_at(t), mixed_at(t), mix_recv.at[t // 2]).wait()

    @pl.loop(0, n_sp)
    def _(k):
        to = lax.rem(e + n_sp - k, n_sp)
        place = to * capacity + lax.broadcasted_iota(jnp.int32, (capacity, tokens), 0)
        named = place == slot_rows[0:1]
        for r in range(1, slot_rows.shape[0]):
            named = named | (place == slot_rows[r : r + 1])
        picks = jnp.where(named, 1.0, 0.0).astype(mixed.dtype)
        outgoing[to] = jnp.dot(picks, mixed[...], preferred_element_type=jnp.float32).astype(
            outgoing.dtype
        )

        @pl.when(k > 0)
        def _():
            dispatch(k).start()

    own_in = pltpu.make_async_copy(outgoing.at[e], rows_at(e, core), own_sem.at[0])
    own_in.start()

    def near_rows(s):
        return pltpu.make_async_remote_copy(
            src_ref=rows_at(s, core),
            dst_ref=rows_at(s, core),
            send_sem=rows_near.at[s],
            recv_sem=rows_recv.at[s, core],
            device_id=(e, sibling),
            device_id_type=MESH,
        )

    def combine(x):
        for r in range(slot_cols.shape[1]):
            place = x * capacity + lax.broadcasted_iota(jnp.int32, (tokens, capacity), 1)
            picks = jnp.where(place == slot_cols[:, r : r + 1], 1.0, 0.0).astype(mixed.dtype)
            got = jnp.dot(picks, returned[x], preferred_element_type=jnp.float32)
            total[...] += route[:, r : r + 1] * got

    tile = min(256, ff_local)
    out_tile = min(256, width)

    def up_step(s):
        @pl.loop(0, ff_local // tile)
        def _(i):
            at = pl.ds(pl.multiple_of(i * tile, tile), tile)
            g = jnp.dot(rows[s], gate_v[:, at], preferred_element_type=jnp.float32)
            u = jnp.dot(rows[s], up_v[:, at], preferred_element_type=jnp.float32)
            h = (g / (1.0 + jnp.exp(-g)) * u).astype(hidden.dtype)
            hidden[s, :, pl.ds(pl.multiple_of(q * ff_local + i * tile, tile), tile)] = h

    def down_step(s):
        @pl.loop(0, width // out_tile)
        def _(i):
            at = pl.ds(pl.multiple_of(i * out_tile, out_tile), out_tile)
            o = jnp.dot(hidden[s], down_v[:, at], preferred_element_type=jnp.float32)
            results[s, :, at] = o.astype(results.dtype)

    @pl.loop(0, n_sp + 3)
    def _(i):
        @pl.when(i < n_sp)
        def _():
            @pl.when(i == 0)
            def _():
                own_in.wait()

            @pl.when(i > 0)
            def _():
                arrived(rows_at, rows_recv, source(i), core)

            near_rows(source(i)).start()

        @pl.when((i >= 1) & (i < n_sp + 1))
        def _():
            s = source(i - 1)
            arrived(rows_at, rows_recv, s, 1 - core)

            @pl.when(i == 1)
            def _():
                for load in loads:
                    load.wait()

            up_step(s)
            spread(hidden_at, hid_recv, hid_far, hid_near, s)

        @pl.when((i >= 2) & (i < n_sp + 2))
        def _():
            relay(hidden_at, hid_recv, hid_near, source(i - 2))

        @pl.when(i >= 3)
        def _():
            s = source(i - 3)
            collect(hidden_at, hid_recv, s)
            down_step(s)

            @pl.when(i == 3)
            def _():
                pltpu.make_async_copy(results.at[e], returned.at[e], own_sem.at[1]).start()

            @pl.when(i > 3)
            def _():
                give_back(i - 3).start()

    pltpu.make_async_copy(results.at[e], returned.at[e], own_sem.at[1]).wait()
    combine(e)

    @pl.loop(1, n_sp)
    def _(k):
        x = lax.rem(e + n_sp - k, n_sp)
        pltpu.make_async_copy(returned.at[x], returned.at[x], ret_recv.at[x]).wait()
        combine(x)

    out[...] = (mixed[:, own_columns].astype(jnp.float32) + total[...]).astype(out.dtype)

    for o in range(1, n_tp):
        tell(o).wait_send()
    for j in range(1, n_y):
        cross(j).wait_send()
    drain(act_at, act_recv, act_far, act_near, 0)

    @pl.loop(0, n_sp)
    def _(s):
        near_rows(s).wait_send()
        drain(hidden_at, hid_recv, hid_far, hid_near, s)

    @pl.loop(1, n_sp)
    def _(k):
        dispatch(k).wait_send()
        give_back(k).wait_send()


def run_layer(filtered, gain, proj, resid, slot_rows, slot_cols, route, w_gate, w_up, w_down):
    n_sp, n_tp = lax.axis_size("sp"), lax.axis_size("tp")
    n_y = n_tp // 2
    tokens, width = resid.shape
    capacity = 4 * tokens // n_sp
    ff_local = w_gate.shape[2]
    dma = pltpu.SemaphoreType.DMA
    vmem = pl.BlockSpec(memory_space=pltpu.VMEM)
    return pl.pallas_call(
        functools.partial(expert_kernel, n_sp, n_tp),
        out_shape=jax.ShapeDtypeStruct(resid.shape, resid.dtype),
        in_specs=[vmem] * 7 + [pl.BlockSpec(memory_space=pl.ANY)] * 3,
        out_specs=vmem,
        scratch_shapes=[
            pltpu.VMEM((n_tp, 8, tokens), jnp.float32),
            pltpu.VMEM((n_tp,) + filtered.shape, jnp.bfloat16),
            pltpu.VMEM((tokens, n_y * width), jnp.bfloat16),
            pltpu.VMEM((tokens, width), jnp.float32),
            pltpu.VMEM((n_sp, capacity, n_y * width), jnp.bfloat16),
            pltpu.VMEM((n_sp, capacity, width * n_tp), jnp.bfloat16),
            pltpu.VMEM((n_sp, capacity, ff_local * n_tp), jnp.bfloat16),
            pltpu.VMEM((n_sp, capacity, width), jnp.bfloat16),
            pltpu.VMEM((n_sp, capacity, width), jnp.bfloat16),
            pltpu.VMEM(w_gate.shape[1:], jnp.bfloat16),
            pltpu.VMEM(w_up.shape[1:], jnp.bfloat16),
            pltpu.VMEM(w_down.shape[1:], jnp.bfloat16),
            dma((3, n_tp)),
            dma((2,)),
            dma((n_tp,)),
            dma((n_tp,)),
            dma((1, n_tp)),
            dma((1, n_y)),
            dma((1, n_y)),
            dma((n_y,)),
            dma((n_y,)),
            dma((n_sp,)),
            dma((n_sp, 2)),
            dma((n_sp,)),
            dma((n_sp, n_tp)),
            dma((n_sp, n_y)),
            dma((n_sp, n_y)),
            dma((n_sp,)),
            dma((n_sp,)),
        ],
        compiler_params=pltpu.CompilerParams(
            collective_id=0, has_side_effects=True, vmem_limit_bytes=52 * 1024 * 1024
        ),
    )(filtered, gain, proj, resid, slot_rows, slot_cols, route, w_gate, w_up, w_down)


def from_behind(block, axis, distance):
    devices = range(lax.axis_size(axis))
    route = [(i - distance, i) for i in devices if i - distance in devices]
    return lax.ppermute(block, axis, route)


def per_device(
    glu_value,
    glu_gate,
    conv_taps,
    norm_gain,
    out_proj,
    resid,
    expert_ids,
    route_logits,
    group_prob,
    w_gate,
    w_up,
    w_down,
):
    local_tokens = glu_value.shape[1]
    tap_count = conv_taps.shape[1]
    gated = (glu_value.astype(jnp.float32) * jax.nn.sigmoid(glu_gate.astype(jnp.float32))).astype(
        jnp.bfloat16
    )
    history = from_behind(gated[:, local_tokens - (tap_count - 1) :], "sp", 1)
    padded = jnp.concatenate([history, gated], axis=1).astype(jnp.float32)
    filtered = jnp.zeros(gated.shape, jnp.float32)
    for offset in range(tap_count):
        filtered = (
            filtered + conv_taps[:, offset : offset + 1] * padded[:, offset : offset + local_tokens]
        )
    experts = lax.axis_size("sp")
    capacity = 4 * local_tokens // experts
    flat_ids = expert_ids.reshape(-1)
    onehot = (flat_ids[:, None] == jnp.arange(experts, dtype=jnp.int32)[None, :]).astype(jnp.int32)
    rank = jnp.sum(jnp.cumsum(onehot, axis=0) * onehot, axis=1) - 1
    slot = flat_ids * capacity + rank
    slots = slot.reshape(expert_ids.shape)
    route_weight = group_prob[:, None] * jax.nn.softmax(route_logits, axis=-1)
    return run_layer(
        filtered,
        norm_gain[:, None],
        out_proj,
        resid,
        slots.T,
        slots,
        route_weight,
        w_gate,
        w_up,
        w_down,
    )


def solution(mesh):
    return jax.shard_map(
        per_device,
        mesh=mesh,
        in_specs=(
            P("tp", "sp"),
            P("tp", "sp"),
            P("tp", None),
            P("tp"),
            P(None, "tp"),
            P("sp", "tp"),
            P("sp", None),
            P("sp", None),
            P("sp"),
            P("sp", None, "tp"),
            P("sp", None, "tp"),
            P("sp", None, "tp"),
        ),
        out_specs=P("sp", "tp"),
        check_vma=False,
    )
```

time: 134 us -> 129 us (0.963)
  Pallas kernels: 89.1 us -> 109 us
  blocking collectives: 13.1 us -> 0 us
  local copies, waits for them, and re-layouts: 12.8 us -> 5.41 us
  other arithmetic: 12.9 us -> 9.52 us
    pallas_call x1, Pallas kernels: 89.1 us -> 109 us  [run_layer(): pl.pallas_call(functools.partial(expert_kernel, n_sp, n_tp), out_shape=ja...]
    all_gather x1 -> x0, blocking collectives: 6.74 us -> none  [per_device(): lax.all_gather(activated, 'tp', axis=0, tiled=True)]
    psum x1 -> x0, blocking collectives: 6.33 us -> none  [per_device(): lax.psum((jnp.sum(filtered, axis=0), jnp.sum(filtered * filtered, axis=0)...]
    gather x3 -> x0, local copies, waits for them, and re-layouts: 6.14 us -> none  [the longest x1 3.97 us: per_device(): jnp.take(mixed, table, axis=0).reshape(experts, capacity, mixed.shape[1])]
    reduce_sum x3 -> x1, other arithmetic: 6.42 us -> 0.7 us  [per_device(): route_weight = group_prob[:, None] * jax.nn.softmax(route_logits, axis=-1)]
    add x0 -> x2, other arithmetic: none -> 3.53 us  [the longest x1 3.51 us: per_device(): filtered + conv_taps[:, offset:offset + 1] * padded[:, offset:offset + lo...]
    scatter x1 -> x0, local copies, waits for them, and re-layouts: 2.45 us -> none  [per_device(): table = jnp.zeros((experts * capacity,), jnp.int32).at[slot].set(token_of)]
  transfers between devices with their start and end apart: 1 -> 1, of which waited for: 0 -> 0; matrix products, arithmetic and copies ran while one was open for 9% -> 7% of each run, Pallas kernels for 0% -> 0%
where the time goes in v2:
time: 129 us
  Pallas kernels  109 us (84%)
  other arithmetic  9.52 us (7%)
  local copies, waits for them, and re-layouts  5.41 us (4%)
  starting transfers between devices  4.87 us (4%)
    pallas_call x1, Pallas kernels, run_layer(): pl.pallas_call(functools.partial(expert_kernel, n_sp, n_tp), out_shape=ja...  109 us
    ppermute x1, starting transfers between devices, from_behind(): return lax.ppermute(block, axis, route)  4.87 us
    add x1, other arithmetic, per_device(): filtered + conv_taps[:, offset:offset + 1] * padded[:, offset:offset + lo...  3.51 us
  transfers between devices with their start and end apart: 1, of which 0 were waited for; matrix products, arithmetic and copies ran while one was open for 7% of the time, Pallas kernels for 0%

profile of v2, /device:TPU:0, one launch (start us, length us, event | category | flops | bytes accessed | tf_op | source)
XLA Modules:
  0.0 129.0 jit_solution(11775626604537567083)
XLA Ops:
  0.0 1.0 multiply_convert_fusion
  1.0 0.1 slice.260
  1.1 4.9 %collective-permute-start = (bf16[256,30]{1,0:T(8,128)(2,1)S(1)}, bf16[256,30]{1,0:T(8,128)(2,1)S(1)}, u32[]{:S(2)}, u32[]{:S(2)}) collective-permute-start(bf16[256,30]{1,0:T(8,128)(2,1)S(1)} %slice.260), channel_id=1, source_target_pairs={{0,4},{4,8},{8,12},{12,16},{16,20},{20,24},{24,28},{1,5},{5,9},{9,... | collective-permute-start | bytes 46088 | tf_op jit(solution)/shard_map/ppermute | solution.py:407
  6.0 1.0 fusion.34
  7.0 1.0 fusion.35
  8.0 0.8 copy.30
  8.8 0.1 eq.29
  9.0 0.1 eq.25
  9.1 0.7 broadcast_multiply_fusion.1
  9.8 1.1 reduce-window.6
  11.0 0.2 slice_reduce_fusion
  11.2 0.7 reduce_max.9
  11.9 0.7 fusion.33
  12.6 0.7 fusion.32
  13.3 0.1 copy.35
  13.5 0.1 fusion.30
  13.6 0.8 broadcast_multiply_fusion.route
  14.3 0.1 sub.15
  14.5 0.1 copy.32
  14.7 0.1 copy.37.slot_rows
  14.7 0.8 copy.36.gain
  15.6 0.0 collective-permute-done
  15.6 0.1 maximum_convert_fusion
  15.7 0.0 copy-start
  15.7 3.5 %fusion.filtered = f32[256,256]{1,0:T(8,128)S(1)} fusion(f32[256,286]{1,0:T(8,128)S(1)} %maximum_convert_fusion, f32[256]{0:T(256)S(1)} %bitcast.69, f32[256]{0:T(256)S(1)} %bitcast.70, f32[256]{0:T(256)S(1)} %bitcast.41, f32[256]{0:T(256)S(1)} %bitcast.42, f32[256]{0:T(256)S(1)} %bitcast.43, f32[256]{0:T(256)S(1)} %bitcast.44, f32[256]{0:T(256)S(1)} %bitcast.45, ...), kind=kLoop, calls=%fused_computation.1 | loop fusion | flops 3997696 | bytes 8420352 | tf_op jit(solution)/shard_map/add | solution.py:434
  19.2 0.0 copy-done
  19.2 109.1 %shard_map.118 = bf16[256,512]{1,0:T(8,128)(2,1)S(1)} custom-call(f32[256,256]{1,0:T(8,128)S(1)} %fusion.filtered, f32[256,1]{1,0:T(8,128)S(1)} %copy.36.gain, bf16[1024,512]{1,0:T(8,128)(2,1)} %proj.1, bf16[256,512]{1,0:T(8,128)(2,1)S(1)} %copy-done, s32[2,256]{1,0:T(2,128)S(1)} %copy.37.slot_rows, s32[256,2]{1,0:T(8,128)S(1)} %add.131.slot_cols, ...), custom_call_target="tpu_custom_call" | custom-call | tf_op jit(solution)/shard_map/pallas_call | solution.py:362
  128.3 0.7 copy.40
  (5 shorter events, 0.1 us)
Async XLA Ops:
  1.1 14.4 %collective-permute-start = (bf16[256,30]{1,0:T(8,128)(2,1)S(1)}, bf16[256,30]{1,0:T(8,128)(2,1)S(1)}, u32[]{:S(2)}, u32[]{:S(2)}) collective-permute-start(bf16[256,30]{1,0:T(8,128)(2,1)S(1)} %slice.260), channel_id=1, source_target_pairs={{0,4},{4,8},{8,12},{12,16},{16,20},{20,24},{24,28},{1,5},{5,9},{9,... | collective-permute-start | bytes 46088 | tf_op jit(solution)/shard_map/ppermute | solution.py:407
  15.7 3.5 %copy-start = (bf16[256,512]{1,0:T(8,128)(2,1)S(1)}, bf16[256,512]{1,0:T(8,128)(2,1)}, u32[]{:S(2)}) copy-start(bf16[256,512]{1,0:T(8,128)(2,1)} %resid.1) | copy-start | bytes 786436

commit v3 on v2

--- a/solution.py
+++ b/solution.py
@@ -17,9 +17,10 @@
     gain,
     proj,
     resid,
-    slot_rows,
-    slot_cols,
-    route,
+    id_rows,
+    id_cols,
+    logits,
+    prob,
     w_gate,
     w_up,
     w_down,
@@ -27,6 +28,8 @@
     stats,
     act,
     mixed,
+    slots,
+    route,
     total,
     outgoing,
     rows,
@@ -43,10 +46,9 @@
     act_recv,
     act_far,
     act_near,
-    mix_send,
-    mix_recv,
     out_send,
     rows_recv,
+    rows_far,
     rows_near,
     hid_recv,
     hid_far,
@@ -60,21 +62,28 @@
     y, core = q // 2, q % 2
     sibling = 2 * y + (1 - core)
     _, capacity, width = results.shape
-    wide = n_y * width
     tokens = mixed.shape[0]
     ff_local = gate_v.shape[1]
 
     def source(k):
-        return lax.rem(e + k, n_sp)
-
-    def rows_at(s, c):
-        return rows.at[s, :, pl.ds(pl.multiple_of(c * wide, wide), wide)]
+        if n_sp & (n_sp - 1) or n_sp == 1:
+            return lax.rem(e + k, n_sp)
+        k = jnp.where(k == 0, 0, lax.rem(k, n_sp - 1) + 1) if n_sp > 2 else k
+        at, bit = 0, 1
+        while bit < n_sp:
+            at, bit = at + (e // bit + k // bit) % 2 * bit, 2 * bit
+        return at
+
+    def target(k):
+        if n_sp & (n_sp - 1) or n_sp == 1:
+            return lax.rem(e + n_sp - k, n_sp)
+        return source(k)
+
+    def rows_at(s, t):
+        return rows.at[s, :, pl.ds(pl.multiple_of(t * width, width), width)]
 
     def act_at(s, t):
         return act.at[t]
-
-    def mixed_at(t):
-        return mixed.at[:, pl.ds(pl.multiple_of((t // 2) * width, width), width)]
 
     def hidden_at(s, t):
         return hidden.at[s, :, pl.ds(pl.multiple_of(t * ff_local, ff_local), ff_local)]
@@ -96,12 +105,12 @@
         )
 
     def dispatch(k):
-        to = lax.rem(e + n_sp - k, n_sp)
+        to = target(k)
         return pltpu.make_async_remote_copy(
             src_ref=outgoing.at[to],
-            dst_ref=rows_at(e, core),
+            dst_ref=rows_at(e, q),
             send_sem=out_send.at[k],
-            recv_sem=rows_recv.at[e, core],
+            recv_sem=rows_recv.at[e, q],
             device_id=(to, q),
             device_id_type=MESH,
         )
@@ -130,23 +139,11 @@
             device_id_type=MESH,
         )
 
-    def cross(j):
-        return pltpu.make_async_remote_copy(
-            src_ref=mixed_at(q),
-            dst_ref=mixed_at(q),
-            send_sem=mix_send.at[j],
-            recv_sem=mix_recv.at[y],
-            device_id=(e, far(j)),
-            device_id_type=MESH,
-        )
-
-    loads = [pltpu.make_async_copy(w_down.at[0], down_v, load_sem.at[2, 0])]
-    for t in range(n_tp):
-        to = pl.ds((t % 2 * n_y + t // 2) * width, width)
-        at = pl.ds(t * width, width)
-        loads.append(pltpu.make_async_copy(w_gate.at[0, at], gate_v.at[to], load_sem.at[0, t]))
-        loads.append(pltpu.make_async_copy(w_up.at[0, at], up_v.at[to], load_sem.at[1, t]))
-
+    loads = [
+        pltpu.make_async_copy(w_gate.at[0], gate_v, load_sem.at[0]),
+        pltpu.make_async_copy(w_up.at[0], up_v, load_sem.at[1]),
+        pltpu.make_async_copy(w_down.at[0], down_v, load_sem.at[2]),
+    ]
     barrier = pltpu.get_barrier_semaphore()
 
     @pl.loop(1, n_sp)
@@ -160,6 +157,36 @@
     for load in loads:
         load.start()
 
+    top = id_rows.shape[0]
+    ahead = lax.broadcasted_iota(jnp.int32, (tokens, tokens), 0)
+    after = lax.broadcasted_iota(jnp.int32, (tokens, tokens), 1)
+    lanes = max(128, n_sp)
+    row_no = lax.broadcasted_iota(jnp.int32, (lanes, tokens), 0)
+    col_no = lax.broadcasted_iota(jnp.int32, (tokens, lanes), 1)
+    row_hit = [jnp.where(row_no == id_rows[r : r + 1], 1.0, 0.0) for r in range(top)]
+    col_hit = [jnp.where(col_no == id_cols[:, r : r + 1], 1.0, 0.0) for r in range(top)]
+    row_rank = jnp.dot(
+        sum(row_hit).astype(jnp.bfloat16),
+        jnp.where(ahead < after, 1.0, 0.0).astype(jnp.bfloat16),
+        preferred_element_type=jnp.float32,
+    )
+    col_rank = jnp.dot(
+        jnp.where(ahead > after, 1.0, 0.0).astype(jnp.bfloat16),
+        sum(col_hit).astype(jnp.bfloat16),
+        preferred_element_type=jnp.float32,
+    )
+    slot_rows = [
+        (id_rows[r : r + 1] * capacity).astype(jnp.float32)
+        + jnp.sum(row_hit[r] * row_rank, axis=0, keepdims=True)
+        for r in range(top)
+    ]
+    for r in range(top):
+        slots[:, r : r + 1] = (id_cols[:, r : r + 1] * capacity).astype(jnp.float32) + jnp.sum(
+            col_hit[r] * col_rank, axis=1, keepdims=True
+        )
+    scores = logits[...]
+    scores = jnp.exp(scores - jnp.max(scores, axis=1, keepdims=True))
+    route[...] = prob[...] * scores / jnp.sum(scores, axis=1, keepdims=True)
     raw = filtered[...]
     stats[q, 0:1] = jnp.sum(raw, axis=0, keepdims=True)
     stats[q, 1:2] = jnp.sum(raw * raw, axis=0, keepdims=True)
@@ -214,48 +241,35 @@
             (((0,), (0,)), ((), ())),
             preferred_element_type=jnp.float32,
         )
-    own_columns = pl.ds(pl.multiple_of(y * width, width), width)
-    mixed[:, own_columns] = sums.astype(mixed.dtype)
-    for j in range(1, n_y):
-        cross(j).start()
-    total[...] = jnp.zeros_like(total)
-    for j in range(1, n_y):
-        t = behind(j)
-        pltpu.make_async_copy(mixed_at(t), mixed_at(t), mix_recv.at[t // 2]).wait()
+    mixed[...] = sums.astype(mixed.dtype)
 
     @pl.loop(0, n_sp)
     def _(k):
-        to = lax.rem(e + n_sp - k, n_sp)
-        place = to * capacity + lax.broadcasted_iota(jnp.int32, (capacity, tokens), 0)
-        named = place == slot_rows[0:1]
-        for r in range(1, slot_rows.shape[0]):
-            named = named | (place == slot_rows[r : r + 1])
-        picks = jnp.where(named, 1.0, 0.0).astype(mixed.dtype)
-        outgoing[to] = jnp.dot(picks, mixed[...], preferred_element_type=jnp.float32).astype(
-            outgoing.dtype
-        )
+        to = target(k)
+        place = (to * capacity + lax.broadcasted_iota(jnp.int32, (capacity, tokens), 0)).astype(
+            jnp.float32
+        )
+        picks = jnp.zeros((capacity, tokens), jnp.float32)
+        for r in range(top):
+            picks = picks + jnp.where(place == slot_rows[r], 1.0, 0.0)
+        outgoing[to] = jnp.dot(
+            picks.astype(mixed.dtype), mixed[...], preferred_element_type=jnp.float32
+        ).astype(outgoing.dtype)
 
         @pl.when(k > 0)
         def _():
             dispatch(k).start()
 
-    own_in = pltpu.make_async_copy(outgoing.at[e], rows_at(e, core), own_sem.at[0])
+    total[...] = jnp.zeros_like(total)
+    own_in = pltpu.make_async_copy(outgoing.at[e], rows_at(e, q), own_sem.at[0])
     own_in.start()
 
-    def near_rows(s):
-        return pltpu.make_async_remote_copy(
-            src_ref=rows_at(s, core),
-            dst_ref=rows_at(s, core),
-            send_sem=rows_near.at[s],
-            recv_sem=rows_recv.at[s, core],
-            device_id=(e, sibling),
-            device_id_type=MESH,
-        )
-
     def combine(x):
-        for r in range(slot_cols.shape[1]):
-            place = x * capacity + lax.broadcasted_iota(jnp.int32, (tokens, capacity), 1)
-            picks = jnp.where(place == slot_cols[:, r : r + 1], 1.0, 0.0).astype(mixed.dtype)
+        place = (x * capacity + lax.broadcasted_iota(jnp.int32, (tokens, capacity), 1)).astype(
+            jnp.float32
+        )
+        for r in range(top):
+            picks = jnp.where(place == slots[:, r : r + 1], 1.0, 0.0).astype(mixed.dtype)
             got = jnp.dot(picks, returned[x], preferred_element_type=jnp.float32)
             total[...] += route[:, r : r + 1] * got
 
@@ -278,7 +292,7 @@
             o = jnp.dot(hidden[s], down_v[:, at], preferred_element_type=jnp.float32)
             results[s, :, at] = o.astype(results.dtype)
 
-    @pl.loop(0, n_sp + 3)
+    @pl.loop(0, n_sp + 4)
     def _(i):
         @pl.when(i < n_sp)
         def _():
@@ -288,16 +302,20 @@
 
             @pl.when(i > 0)
             def _():
-                arrived(rows_at, rows_recv, source(i), core)
-
-            near_rows(source(i)).start()
+                arrived(rows_at, rows_recv, source(i), q)
+
+            spread(rows_at, rows_recv, rows_far, rows_near, source(i))
 
         @pl.when((i >= 1) & (i < n_sp + 1))
         def _():
-            s = source(i - 1)
-            arrived(rows_at, rows_recv, s, 1 - core)
-
-            @pl.when(i == 1)
+            relay(rows_at, rows_recv, rows_near, source(i - 1))
+
+        @pl.when((i >= 2) & (i < n_sp + 2))
+        def _():
+            s = source(i - 2)
+            collect(rows_at, rows_recv, s)
+
+            @pl.when(i == 2)
             def _():
                 for load in loads:
                     load.wait()
@@ -305,44 +323,42 @@
             up_step(s)
             spread(hidden_at, hid_recv, hid_far, hid_near, s)
 
-        @pl.when((i >= 2) & (i < n_sp + 2))
-        def _():
-            relay(hidden_at, hid_recv, hid_near, source(i - 2))
-
-        @pl.when(i >= 3)
-        def _():
-            s = source(i - 3)
+        @pl.when((i >= 3) & (i < n_sp + 3))
+        def _():
+            relay(hidden_at, hid_recv, hid_near, source(i - 3))
+
+        @pl.when(i >= 4)
+        def _():
+            s = source(i - 4)
             collect(hidden_at, hid_recv, s)
             down_step(s)
 
-            @pl.when(i == 3)
+            @pl.when(i == 4)
             def _():
                 pltpu.make_async_copy(results.at[e], returned.at[e], own_sem.at[1]).start()
 
-            @pl.when(i > 3)
+            @pl.when(i > 4)
             def _():
-                give_back(i - 3).start()
+                give_back(i - 4).start()
 
     pltpu.make_async_copy(results.at[e], returned.at[e], own_sem.at[1]).wait()
     combine(e)
 
     @pl.loop(1, n_sp)
     def _(k):
-        x = lax.rem(e + n_sp - k, n_sp)
+        x = target(k)
         pltpu.make_async_copy(returned.at[x], returned.at[x], ret_recv.at[x]).wait()
         combine(x)
 
-    out[...] = (mixed[:, own_columns].astype(jnp.float32) + total[...]).astype(out.dtype)
+    out[...] = (mixed[...].astype(jnp.float32) + total[...]).astype(out.dtype)
 
     for o in range(1, n_tp):
         tell(o).wait_send()
-    for j in range(1, n_y):
-        cross(j).wait_send()
     drain(act_at, act_recv, act_far, act_near, 0)
 
     @pl.loop(0, n_sp)
     def _(s):
-        near_rows(s).wait_send()
+        drain(rows_at, rows_recv, rows_far, rows_near, s)
         drain(hidden_at, hid_recv, hid_far, hid_near, s)
 
     @pl.loop(1, n_sp)
@@ -351,7 +367,7 @@
         give_back(k).wait_send()
 
 
-def run_layer(filtered, gain, proj, resid, slot_rows, slot_cols, route, w_gate, w_up, w_down):
+def run_layer(filtered, gain, proj, resid, id_rows, id_cols, logits, prob, w_gate, w_up, w_down):
     n_sp, n_tp = lax.axis_size("sp"), lax.axis_size("tp")
     n_y = n_tp // 2
     tokens, width = resid.shape
@@ -362,14 +378,16 @@
     return pl.pallas_call(
         functools.partial(expert_kernel, n_sp, n_tp),
         out_shape=jax.ShapeDtypeStruct(resid.shape, resid.dtype),
-        in_specs=[vmem] * 7 + [pl.BlockSpec(memory_space=pl.ANY)] * 3,
+        in_specs=[vmem] * 8 + [pl.BlockSpec(memory_space=pl.ANY)] * 3,
         out_specs=vmem,
         scratch_shapes=[
             pltpu.VMEM((n_tp, 8, tokens), jnp.float32),
             pltpu.VMEM((n_tp,) + filtered.shape, jnp.bfloat16),
-            pltpu.VMEM((tokens, n_y * width), jnp.bfloat16),
+            pltpu.VMEM((tokens, width), jnp.bfloat16),
+            pltpu.VMEM((tokens, id_cols.shape[1]), jnp.float32),
+            pltpu.VMEM((tokens, id_cols.shape[1]), jnp.float32),
             pltpu.VMEM((tokens, width), jnp.float32),
-            pltpu.VMEM((n_sp, capacity, n_y * width), jnp.bfloat16),
+            pltpu.VMEM((n_sp, capacity, width), jnp.bfloat16),
             pltpu.VMEM((n_sp, capacity, width * n_tp), jnp.bfloat16),
             pltpu.VMEM((n_sp, capacity, ff_local * n_tp), jnp.bfloat16),
             pltpu.VMEM((n_sp, capacity, width), jnp.bfloat16),
@@ -377,18 +395,17 @@
             pltpu.VMEM(w_gate.shape[1:], jnp.bfloat16),
             pltpu.VMEM(w_up.shape[1:], jnp.bfloat16),
             pltpu.VMEM(w_down.shape[1:], jnp.bfloat16),
-            dma((3, n_tp)),
+            dma((3,)),
             dma((2,)),
             dma((n_tp,)),
             dma((n_tp,)),
             dma((1, n_tp)),
             dma((1, n_y)),
             dma((1, n_y)),
-            dma((n_y,)),
-            dma((n_y,)),
             dma((n_sp,)),
-            dma((n_sp, 2)),
-            dma((n_sp,)),
+            dma((n_sp, n_tp)),
+            dma((n_sp, n_y)),
+            dma((n_sp, n_y)),
             dma((n_sp, n_tp)),
             dma((n_sp, n_y)),
             dma((n_sp, n_y)),
@@ -398,7 +415,7 @@
         compiler_params=pltpu.CompilerParams(
             collective_id=0, has_side_effects=True, vmem_limit_bytes=52 * 1024 * 1024
         ),
-    )(filtered, gain, proj, resid, slot_rows, slot_cols, route, w_gate, w_up, w_down)
+    )(filtered, gain, proj, resid, id_rows, id_cols, logits, prob, w_gate, w_up, w_down)
 
 
 def from_behind(block, axis, distance):
@@ -433,22 +450,15 @@
         filtered = (
             filtered + conv_taps[:, offset : offset + 1] * padded[:, offset : offset + local_tokens]
         )
-    experts = lax.axis_size("sp")
-    capacity = 4 * local_tokens // experts
-    flat_ids = expert_ids.reshape(-1)
-    onehot = (flat_ids[:, None] == jnp.arange(experts, dtype=jnp.int32)[None, :]).astype(jnp.int32)
-    rank = jnp.sum(jnp.cumsum(onehot, axis=0) * onehot, axis=1) - 1
-    slot = flat_ids * capacity + rank
-    slots = slot.reshape(expert_ids.shape)
-    route_weight = group_prob[:, None] * jax.nn.softmax(route_logits, axis=-1)
     return run_layer(
         filtered,
         norm_gain[:, None],
         out_proj,
         resid,
-        slots.T,
-        slots,
-        route_weight,
+        expert_ids.T,
+        expert_ids,
+        route_logits,
+        group_prob[:, None],
         w_gate,
         w_up,
         w_down,

time: 129 us -> 119 us (0.922)
  Pallas kernels: 109 us -> 103 us
  other arithmetic: 9.52 us -> 4.68 us
    pallas_call x1, Pallas kernels: 109 us -> 103 us  [run_layer(): pl.pallas_call(functools.partial(expert_kernel, n_sp, n_tp), out_shape=ja...]
    mul x2 -> x0, other arithmetic: 1.47 us -> none  [the longest x1 0.78 us: per_device(): route_weight = group_prob[:, None] * jax.nn.softmax(route_logits, axis=-1)]
  transfers between devices with their start and end apart: 1 -> 1, of which waited for: 0 -> 0; matrix products, arithmetic and copies ran while one was open for 7% -> 4% of each run, Pallas kernels for 0% -> 0%
where the time goes in v3:
time: 119 us
  Pallas kernels  103 us (87%)
  local copies, waits for them, and re-layouts  6.05 us (5%)
  starting transfers between devices  4.87 us (4%)
  other arithmetic  4.68 us (4%)
    pallas_call x1, Pallas kernels, run_layer(): pl.pallas_call(functools.partial(expert_kernel, n_sp, n_tp), out_shape=ja...  103 us
    ppermute x1, starting transfers between devices, from_behind(): return lax.ppermute(block, axis, route)  4.87 us
    add x1, other arithmetic, per_device(): filtered + conv_taps[:, offset:offset + 1] * padded[:, offset:offset + lo...  3.51 us
  transfers between devices with their start and end apart: 1, of which 0 were waited for; matrix products, arithmetic and copies ran while one was open for 4% of the time, Pallas kernels for 0%

profile of v3, /device:TPU:0, one launch (start us, length us, event | category | flops | bytes accessed | tf_op | source)
XLA Modules:
  0.0 118.9 jit_solution(7813659962865289738)
XLA Ops:
  0.0 1.0 multiply_convert_fusion
  1.0 0.1 slice.252
  1.1 4.9 %collective-permute-start = (bf16[256,30]{1,0:T(8,128)(2,1)S(1)}, bf16[256,30]{1,0:T(8,128)(2,1)S(1)}, u32[]{:S(2)}, u32[]{:S(2)}) collective-permute-start(bf16[256,30]{1,0:T(8,128)(2,1)S(1)} %slice.252), channel_id=1, source_target_pairs={{0,4},{4,8},{8,12},{12,16},{16,20},{20,24},{24,28},{1,5},{5,9},{9,... | collective-permute-start | bytes 46088 | tf_op jit(solution)/shard_map/ppermute | solution.py:424
  6.0 1.0 fusion.30
  7.0 1.0 fusion.31
  8.0 0.8 copy.15.gain
  8.8 0.8 copy.16.id_cols
  9.7 0.8 copy.17.logits
  10.5 0.8 copy.18.prob
  11.3 0.0 collective-permute-done
  11.3 0.1 maximum_convert_fusion
  11.4 0.0 copy-start
  11.5 0.0 copy-start.1
  11.5 3.5 %fusion.filtered = f32[256,256]{1,0:T(8,128)S(1)} fusion(f32[256,286]{1,0:T(8,128)S(1)} %maximum_convert_fusion, f32[256]{0:T(256)S(1)} %bitcast.64, f32[256]{0:T(256)S(1)} %bitcast.65, f32[256]{0:T(256)S(1)} %bitcast.36, f32[256]{0:T(256)S(1)} %bitcast.37, f32[256]{0:T(256)S(1)} %bitcast.38, f32[256]{0:T(256)S(1)} %bitcast.39, f32[256]{0:T(256)S(1)} %bitcast.40, ...), kind=kLoop, calls=%fused_computation.1 | loop fusion | flops 3997696 | bytes 8420352 | tf_op jit(solution)/shard_map/add | solution.py:451
  15.0 0.0 copy-done
  15.0 0.0 copy-done.1
  15.0 103.1 %shard_map.118 = bf16[256,512]{1,0:T(8,128)(2,1)S(1)} custom-call(f32[256,256]{1,0:T(8,128)S(1)} %fusion.filtered, f32[256,1]{1,0:T(8,128)S(1)} %copy.15.gain, bf16[1024,512]{1,0:T(8,128)(2,1)} %proj.1, bf16[256,512]{1,0:T(8,128)(2,1)S(1)} %copy-done, s32[2,256]{1,0:T(2,128)S(1)} %bitcast.34, s32[256,2]{1,0:T(8,128)S(1)} %copy.16.id_cols, ...), custom_call_target="tpu_custom_call" | custom-call | tf_op jit(solution)/shard_map/pallas_call | solution.py:378
  118.2 0.7 copy.20
Async XLA Ops:
  1.1 10.2 %collective-permute-start = (bf16[256,30]{1,0:T(8,128)(2,1)S(1)}, bf16[256,30]{1,0:T(8,128)(2,1)S(1)}, u32[]{:S(2)}, u32[]{:S(2)}) collective-permute-start(bf16[256,30]{1,0:T(8,128)(2,1)S(1)} %slice.252), channel_id=1, source_target_pairs={{0,4},{4,8},{8,12},{12,16},{16,20},{20,24},{24,28},{1,5},{5,9},{9,... | collective-permute-start | bytes 46088 | tf_op jit(solution)/shard_map/ppermute | solution.py:424
  11.4 3.5 %copy-start = (bf16[256,512]{1,0:T(8,128)(2,1)S(1)}, bf16[256,512]{1,0:T(8,128)(2,1)}, u32[]{:S(2)}) copy-start(bf16[256,512]{1,0:T(8,128)(2,1)} %resid.1) | copy-start | bytes 786436
  11.5 3.5 %copy-start.1 = (s32[256,2]{0,1:T(2,128)S(1)}, s32[256,2]{0,1:T(2,128)}, u32[]{:S(2)}) copy-start(s32[256,2]{0,1:T(2,128)} %param.18) | copy-start | bytes 6148
